TPU v7x, 32 devices: a whole 2x2x4 slice. The times are simulated.
32 devices in a mesh: fs: 16 (over z, y, x), tp: 2 (over core).
Axes of the slice: x: 2, y: 2, z: 4, core: 2. Of those that a mesh axis runs over, the one named last changes fastest.
Arguments:
- normed_input: bfloat16 [8192, 2048], P('fs', 'tp'), may hold values from -6 to 6
- cotangent: bfloat16 [8192, 2048], P('fs', 'tp'), may hold values from -6 to 6
- up_weight: bfloat16 [2048, 8192], P('fs', 'tp'), may hold values from -0.125 to 0.125
- down_weight: bfloat16 [8192, 2048], P('tp', 'fs'), may hold values from -0.0625 to 0.0625
Outputs:
- input_grad: bfloat16 [8192, 2048], P('fs', 'tp')
- up_grad: float32 [2048, 8192], P('fs', 'tp')
- down_grad: float32 [8192, 2048], P('tp', 'fs')
All inputs are finite; a program needn't handle non-finite values.
Results may differ from a plain program's by a relative error of at most 0.018.
Values may be sent and summed in bfloat16 or wider, within the bound.
A program may use at most 192 MiB of HBM per device.

v0:
```python
import jax
import jax.numpy as jnp
from jax import lax
from jax.sharding import PartitionSpec as P


def right_product(left, right):
    return lax.dot_general(
        left, right, (((1,), (1,)), ((), ())), preferred_element_type=jnp.float32
    )


def left_product(left, right):
    return lax.dot_general(
        left, right, (((0,), (0,)), ((), ())), preferred_element_type=jnp.float32
    )


def per_device(normed_input, cotangent, up_weight, down_weight):
    whole_input, whole_cot = (
        lax.all_gather(normed_input, "tp", axis=1, tiled=True),
        lax.all_gather(cotangent, "tp", axis=1, tiled=True),
    )
    rows = whole_input.shape[0]
    tokens = rows * lax.axis_size("fs")
    scale = lax.rsqrt(jnp.asarray(tokens, jnp.float32))
    block = whole_cot
    act_grad = right_product(block, lax.all_gather(down_weight, "fs", axis=1, tiled=True))
    whole_up = lax.all_gather(up_weight, "fs", axis=0, tiled=True)
    pre = jnp.dot(whole_input, whole_up, preferred_element_type=jnp.float32)
    rectified = jax.nn.relu(pre)
    act = (rectified * rectified).astype(jnp.bfloat16)
    pre_grad = (2.0 * rectified * act_grad).astype(jnp.bfloat16)
    partial_value = right_product(pre_grad, whole_up)
    input_grad = lax.psum_scatter(
        partial_value.astype(jnp.bfloat16), "tp", scatter_dimension=1, tiled=True
    )
    block = whole_input
    up_grad = lax.psum_scatter(
        (left_product(block, pre_grad) * scale).astype(jnp.bfloat16),
        "fs",
        scatter_dimension=0,
        tiled=True,
    ).astype(jnp.float32)
    down_term = left_product(act, whole_cot) * scale
    down_grad = lax.psum_scatter(
        down_term.astype(jnp.bfloat16), "fs", scatter_dimension=1, tiled=True
    ).astype(jnp.float32)
    return (input_grad, up_grad, down_grad)


def solution(mesh):
    in_specs = (P("fs", "tp"), P("fs", "tp"), P("fs", "tp"), P("tp", "fs"))
    out_specs = (P("fs", "tp"), P("fs", "tp"), P("tp", "fs"))
    return jax.shard_map(
        per_device, mesh=mesh, in_specs=in_specs, out_specs=out_specs, check_vma=False
    )
```

profile of v0, /device:TPU:0, one launch (start us, length us, event | category | flops | bytes accessed | tf_op | source)
XLA Modules:
  0.0 1207.0 jit_solution(5225547359864163482)
XLA Ops:
  7.2 0.0 all-gather.5.cloned.1.call-start
  7.2 0.7 all-gather.5.cloned.1.call-update
  7.9 0.0 all-gather.7.cloned.1.call-start
  7.9 0.7 all-gather.7.cloned.1.call-update
  8.6 0.0 all-gather.9.cloned.1.call-start
  8.7 0.7 all-gather.9.cloned.1.call-update
  9.4 0.0 all-gather.11.cloned.1.call-start
  9.4 0.5 all-gather.11.cloned.1.call-update
  10.0 0.0 reduce-scatter.12.cloned.1.call-start
  10.0 12.8 %all-gather.5.cloned.1.call-done = bf16[512,2048]{1,0:T(8,128)(2,1)} async-done(((bf16[512,1024]{1,0:T(8,128)(2,1)}), bf16[512,2048]{1,0:T(8,128)(2,1)}) %all-gather.5.cloned.1.call-update) | async-done | bytes 2097168 | tf_op jit(solution)/shard_map/all_gather | solution.py:21
  22.8 195.0 %all-gather.7.cloned.1.call-done = bf16[2048,4096]{1,0:T(8,128)(2,1)} async-done(((bf16[128,4096]{1,0:T(8,128)(2,1)}), bf16[2048,4096]{1,0:T(8,128)(2,1)}) %all-gather.7.cloned.1.call-update) | async-done | bytes 16777232 | tf_op jit(solution)/shard_map/all_gather | solution.py:29
  217.8 14.9 %fusion.3 = f32[512,4096]{1,0:T(8,128)} fusion(bf16[512,2048]{1,0:T(8,128)(2,1)} %all-gather.5.cloned.1.call-done, bf16[2048,4096]{1,0:T(8,128)(2,1)} %all-gather.7.cloned.1.call-done), kind=kOutput, calls=%fused_computation.8 | convolution fusion | flops 8589934592 | bytes 27262976 | tf_op jit(solution)/shard_map/dot_general | solution.py:30
  232.7 0.0 all-gather.9.cloned.1.call-done
  232.7 16.2 %multiply_convert_fusion = bf16[4096,2048]{1,0:T(8,128)(2,1)} fusion(bf16[512,2048]{1,0:T(8,128)(2,1)} %all-gather.9.cloned.1.call-done, f32[512,4096]{1,0:T(8,128)} %fusion.3), kind=kOutput, calls=%fused_computation | convolution fusion | flops 8613003264 | bytes 27262976 | tf_op jit(solution)/shard_map/dot_general | solution.py:14
  248.9 21.5 %copy.11 = bf16[4096,2048]{0,1:T(8,128)(2,1)} copy(bf16[4096,2048]{1,0:T(8,128)(2,1)} %multiply_convert_fusion) | data formatting | bytes 33554432
  270.4 0.0 reduce-scatter.12.cloned.1.call-update
  270.5 0.0 copy-start
  270.5 0.2 reduce-scatter.10.cloned.1.call-start
  270.7 210.3 %all-gather.11.cloned.1.call-done = bf16[4096,2048]{1,0:T(8,128)(2,1)} async-done(((bf16[4096,128]{1,0:T(8,128)(2,1)}), bf16[4096,2048]{1,0:T(8,128)(2,1)}) %all-gather.11.cloned.1.call-update) | async-done | bytes 16777232 | tf_op jit(solution)/shard_map/all_gather | solution.py:28
  481.0 15.6 %multiply_convert_fusion.3 = bf16[512,4096]{1,0:T(8,128)(2,1)} fusion(f32[512,4096]{1,0:T(8,128)} %fusion.3, bf16[512,2048]{1,0:T(8,128)(2,1)} %all-gather.9.cloned.1.call-done, bf16[4096,2048]{1,0:T(8,128)(2,1)} %all-gather.11.cloned.1.call-done), kind=kOutput, calls=%fused_computation.4 | convolution fusion | flops 8598323200 | bytes 31457280 | tf_op jit(solution)/shard_map/dot_general | solution.py:8
  496.6 0.0 copy-done
  496.6 14.8 %fusion = bf16[2048,4096]{0,1:T(8,128)(2,1)} fusion(bf16[512,4096]{1,0:T(8,128)(2,1)} %multiply_convert_fusion.3, bf16[512,2048]{1,0:T(8,128)(2,1)S(1)} %copy-done), kind=kOutput, calls=%fused_computation.2 | convolution fusion | flops 8606711808 | bytes 23068672 | tf_op jit(solution)/shard_map/dot_general | solution.py:14
  511.4 21.4 %copy.9 = bf16[2048,4096]{1,0:T(8,128)(2,1)} copy(bf16[2048,4096]{0,1:T(8,128)(2,1)} %fusion) | data formatting | bytes 33554432
  532.8 0.0 reduce-scatter.10.cloned.1.call-update
  532.8 0.3 reduce-scatter.8.cloned.1.call-start
  533.1 14.8 %convolution_convert_fusion = bf16[512,2048]{1,0:T(8,128)(2,1)} fusion(bf16[512,4096]{1,0:T(8,128)(2,1)} %multiply_convert_fusion.3, bf16[2048,4096]{1,0:T(8,128)(2,1)} %all-gather.7.cloned.1.call-done), kind=kOutput, calls=%fused_computation.6 | convolution fusion | flops 8590983168 | bytes 23068672 | tf_op jit(solution)/shard_map/dot_general | solution.py:8
  547.9 0.0 reduce-scatter.8.cloned.1.call-update
  547.9 279.9 %reduce-scatter.12.cloned.1.call-done = bf16[128,4096]{1,0:T(8,128)(2,1)} async-done(((bf16[2048,4096]{1,0:T(8,128)(2,1)}), bf16[128,4096]{1,0:T(8,128)(2,1)}) %reduce-scatter.12.cloned.1.call-update) | async-done | bytes 1048592
  827.8 1.6 copy.12
  829.4 1.5 convert_element_type.31
  830.9 351.1 %reduce-scatter.10.cloned.1.call-done = bf16[128,4096]{1,0:T(8,128)(2,1)} async-done(((bf16[2048,4096]{1,0:T(8,128)(2,1)}), bf16[128,4096]{1,0:T(8,128)(2,1)}) %reduce-scatter.10.cloned.1.call-update) | async-done | bytes 1048592
  1182.0 1.6 copy.10
  1183.6 1.6 copy.8
  1185.3 14.9 %reduce-scatter.8.cloned.1.call-done = bf16[512,1024]{1,0:T(8,128)(2,1)} async-done(((bf16[512,2048]{1,0:T(8,128)(2,1)}), bf16[512,1024]{1,0:T(8,128)(2,1)}) %reduce-scatter.8.cloned.1.call-update) | async-done | bytes 1048592 | tf_op jit(solution)/shard_map/reduce_scatter | solution.py:35
Async XLA Ops:
  7.2 15.7 %all-gather.5.cloned.1.call-start = ((), (), s32[]{:S(2)}) async-start(), calls=%async_computation.3 | async-start | bytes 3145728 | tf_op jit(solution)/shard_map/all_gather | solution.py:21
  7.9 209.9 %all-gather.7.cloned.1.call-start = ((), (), s32[]{:S(2)}) async-start(), calls=%async_computation.4 | async-start | bytes 17825792 | tf_op jit(solution)/shard_map/all_gather | solution.py:29
  8.6 224.1 %all-gather.9.cloned.1.call-start = ((), (), s32[]{:S(2)}) async-start(), calls=%async_computation.5 | async-start | bytes 3145728 | tf_op jit(solution)/shard_map/all_gather | solution.py:22
  9.4 471.7 %all-gather.11.cloned.1.call-start = ((), (), s32[]{:S(2)}) async-start(), calls=%async_computation.6 | async-start | bytes 17825792 | tf_op jit(solution)/shard_map/all_gather | solution.py:28
  10.0 817.9 %reduce-scatter.12.cloned.1.call-start = ((), (), s32[]{:S(2)}) async-start(), calls=%async_computation.9 | async-start | bytes 17825792
  270.5 226.2 %copy-start = (bf16[512,2048]{1,0:T(8,128)(2,1)S(1)}, bf16[512,2048]{1,0:T(8,128)(2,1)}, u32[]{:S(2)}) copy-start(bf16[512,2048]{1,0:T(8,128)(2,1)} %all-gather.5.cloned.1.call-done) | copy-start | bytes 6291460
  270.5 911.5 %reduce-scatter.10.cloned.1.call-start = ((), (), s32[]{:S(2)}) async-start(), calls=%async_computation.8 | async-start | bytes 17825792
  532.8 667.3 %reduce-scatter.8.cloned.1.call-start = ((), (), s32[]{:S(2)}) async-start(), calls=%async_computation.7 | async-start | bytes 3145728 | tf_op jit(solution)/shard_map/reduce_scatter | solution.py:35
Sparse Core Ops, SparseCore 0:
  9.5 13.2 all-gather.4
  25.6 192.1 all-gather.6
  219.4 8.7 all-gather.8
  230.7 250.2 all-gather.10
  483.2 344.5 reduce-scatter.11
  830.0 352.0 reduce-scatter.9
  1184.8 15.2 reduce-scatter.7
where the time goes:
time: 1210 us
  waiting for transfers between devices  1070 us (88%)
  matrix products  76.2 us (6%)
  local copies, waits for them, and re-layouts  47.8 us (4%)
  between operations  14.2 us (1%)
    unnamed x9, waiting for transfers between devices  634 us
    all_gather x1, waiting for transfers between devices, per_device(): lax.all_gather(down_weight, 'fs', axis=1, tiled=True)  210 us
    all_gather x1, waiting for transfers between devices, per_device(): whole_up = lax.all_gather(up_weight, 'fs', axis=0, tiled=True)  195 us
    unnamed x7, local copies, waits for them, and re-layouts  47.8 us
    dot_general x2, matrix products, left_product(): lax.dot_general(left, right, (((0,), (0,)), ((), ())), preferred_element_...  30.9 us
    dot_general x2, matrix products, right_product(): lax.dot_general(left, right, (((1,), (1,)), ((), ())), preferred_element_...  30.4 us
  transfers between devices with their start and end apart: 7, of which 6 were waited for; matrix products, arithmetic and copies ran while one was open for 10% of the time, Pallas kernels for 0%

commit v1 on v0

--- a/solution.py
+++ b/solution.py
@@ -26,7 +26,12 @@
     scale = lax.rsqrt(jnp.asarray(tokens, jnp.float32))
     block = whole_cot
     act_grad = right_product(block, lax.all_gather(down_weight, "fs", axis=1, tiled=True))
-    whole_up = lax.all_gather(up_weight, "fs", axis=0, tiled=True)
+    ring = [up_weight]
+    for hop in range(15):
+        ring.append(lax.ppermute(ring[-1], "fs", [(dev, (dev + 1) % 16) for dev in range(16)]))
+    whole_up = jnp.roll(
+        jnp.concatenate(ring[::-1], axis=0), (lax.axis_index("fs") + 1) * ring[0].shape[0], axis=0
+    )
     pre = jnp.dot(whole_input, whole_up, preferred_element_type=jnp.float32)
     rectified = jax.nn.relu(pre)
     act = (rectified * rectified).astype(jnp.bfloat16)

time: 1210 us -> 1310 us (1.083)
  local copies, waits for them, and re-layouts: 47.8 us -> 112 us
  waiting for transfers between devices: 1070 us -> 1090 us
  starting transfers between devices: 0.67 us -> 18.6 us
    ppermute x0 -> x15, waiting for transfers between devices: none -> 431 us  [per_device(): lax.ppermute(ring[-1], 'fs', [(dev, (dev + 1) % 16) for dev in range(16)])]
    all_gather x1, waiting for transfers between devices: 210 us -> 0.02 us  [per_device(): lax.all_gather(down_weight, 'fs', axis=1, tiled=True)]
    all_gather x1 -> x0, waiting for transfers between devices: 195 us -> none  [per_device(): whole_up = lax.all_gather(up_weight, 'fs', axis=0, tiled=True)]
    unnamed x7 -> x82, local copies, waits for them, and re-layouts: 47.8 us -> 111 us
    ppermute x0 -> x15, starting transfers between devices: none -> 18.4 us  [per_device(): lax.ppermute(ring[-1], 'fs', [(dev, (dev + 1) % 16) for dev in range(16)])]
    unnamed x9 -> x8, waiting for transfers between devices: 634 us -> 644 us
  transfers between devices with their start and end apart: 7 -> 21, of which waited for: 6 -> 18; matrix products, arithmetic and copies ran while one was open for 10% -> 14% of each run, Pallas kernels for 0% -> 0%
where the time goes in v1:
time: 1310 us
  waiting for transfers between devices  1090 us (83%)
  local copies, waits for them, and re-layouts  112 us (9%)
  matrix products  75.8 us (6%)
  starting transfers between devices  18.6 us (1%)
  between operations  14.3 us (1%)
    unnamed x8, waiting for transfers between devices  644 us
    ppermute x15, waiting for transfers between devices, per_device(): lax.ppermute(ring[-1], 'fs', [(dev, (dev + 1) % 16) for dev in range(16)])  431 us
    unnamed x82, local copies, waits for them, and re-layouts  111 us
    dot_general x2, matrix products, right_product(): lax.dot_general(left, right, (((1,), (1,)), ((), ())), preferred_element_...  32.6 us
    dot_general x2, matrix products, left_product(): lax.dot_general(left, right, (((0,), (0,)), ((), ())), preferred_element_...  27.9 us
  transfers between devices with their start and end apart: 21, of which 18 were waited for; matrix products, arithmetic and copies ran while one was open for 14% of the time, Pallas kernels for 0%

profile of v1, /device:TPU:0, one launch (start us, length us, event | category | flops | bytes accessed | tf_op | source)
XLA Modules:
  0.0 1312.1 jit_solution(5412112724794067305)
XLA Ops:
  8.0 3.0 collective-permute-start
  11.0 27.3 %collective-permute-done = bf16[128,4096]{1,0:T(8,128)(2,1)S(1)} collective-permute-done((bf16[128,4096]{1,0:T(8,128)(2,1)}, bf16[128,4096]{1,0:T(8,128)(2,1)S(1)}, u32[]{:S(2)}, u32[]{:S(2)}) %collective-permute-start) | collective-permute-done | bytes 1048608 | tf_op jit(solution)/shard_map/ppermute | solution.py:31
  38.3 27.9 %collective-permute-done.1 = bf16[128,4096]{1,0:T(8,128)(2,1)S(1)} collective-permute-done((bf16[128,4096]{1,0:T(8,128)(2,1)S(1)}, bf16[128,4096]{1,0:T(8,128)(2,1)S(1)}, u32[]{:S(2)}, u32[]{:S(2)}) %collective-permute-start.1) | collective-permute-done | bytes 1048608 | tf_op jit(solution)/shard_map/ppermute | solution.py:31
  66.3 33.7 %collective-permute-done.2 = bf16[128,4096]{1,0:T(8,128)(2,1)} collective-permute-done((bf16[128,4096]{1,0:T(8,128)(2,1)S(1)}, bf16[128,4096]{1,0:T(8,128)(2,1)}, u32[]{:S(2)}, u32[]{:S(2)}) %collective-permute-start.2) | collective-permute-done | bytes 1048608 | tf_op jit(solution)/shard_map/ppermute | solution.py:31
  100.0 2.6 collective-permute-start.3
  102.6 20.2 %collective-permute-done.3 = bf16[128,4096]{1,0:T(8,128)(2,1)S(1)} collective-permute-done((bf16[128,4096]{1,0:T(8,128)(2,1)}, bf16[128,4096]{1,0:T(8,128)(2,1)S(1)}, u32[]{:S(2)}, u32[]{:S(2)}) %collective-permute-start.3) | collective-permute-done | bytes 1048608 | tf_op jit(solution)/shard_map/ppermute | solution.py:31
  123.8 2.4 collective-permute-start.4
  126.2 20.1 %collective-permute-done.4 = bf16[128,4096]{1,0:T(8,128)(2,1)S(1)} collective-permute-done((bf16[128,4096]{1,0:T(8,128)(2,1)S(1)}, bf16[128,4096]{1,0:T(8,128)(2,1)S(1)}, u32[]{:S(2)}, u32[]{:S(2)}) %collective-permute-start.4) | collective-permute-done | bytes 1048608 | tf_op jit(solution)/shard_map/ppermute | solution.py:31
  147.2 2.3 collective-permute-start.5
  149.5 20.2 %collective-permute-done.5 = bf16[128,4096]{1,0:T(8,128)(2,1)S(1)} collective-permute-done((bf16[128,4096]{1,0:T(8,128)(2,1)S(1)}, bf16[128,4096]{1,0:T(8,128)(2,1)S(1)}, u32[]{:S(2)}, u32[]{:S(2)}) %collective-permute-start.5) | collective-permute-done | bytes 1048608 | tf_op jit(solution)/shard_map/ppermute | solution.py:31
  170.6 2.2 collective-permute-start.6
  172.8 20.3 %collective-permute-done.6 = bf16[128,4096]{1,0:T(8,128)(2,1)S(1)} collective-permute-done((bf16[128,4096]{1,0:T(8,128)(2,1)S(1)}, bf16[128,4096]{1,0:T(8,128)(2,1)S(1)}, u32[]{:S(2)}, u32[]{:S(2)}) %collective-permute-start.6) | collective-permute-done | bytes 1048608 | tf_op jit(solution)/shard_map/ppermute | solution.py:31
  194.1 2.1 collective-permute-start.7
  196.1 20.3 %collective-permute-done.7 = bf16[128,4096]{1,0:T(8,128)(2,1)S(1)} collective-permute-done((bf16[128,4096]{1,0:T(8,128)(2,1)S(1)}, bf16[128,4096]{1,0:T(8,128)(2,1)S(1)}, u32[]{:S(2)}, u32[]{:S(2)}) %collective-permute-start.7) | collective-permute-done | bytes 1048608 | tf_op jit(solution)/shard_map/ppermute | solution.py:31
  217.5 2.0 collective-permute-start.8
  219.5 20.7 %collective-permute-done.8 = bf16[128,4096]{1,0:T(8,128)(2,1)S(1)} collective-permute-done((bf16[128,4096]{1,0:T(8,128)(2,1)S(1)}, bf16[128,4096]{1,0:T(8,128)(2,1)S(1)}, u32[]{:S(2)}, u32[]{:S(2)}) %collective-permute-start.8) | collective-permute-done | bytes 1048608 | tf_op jit(solution)/shard_map/ppermute | solution.py:31
  241.1 1.7 collective-permute-start.9
  242.8 22.1 %collective-permute-done.9 = bf16[128,4096]{1,0:T(8,128)(2,1)S(1)} collective-permute-done((bf16[128,4096]{1,0:T(8,128)(2,1)S(1)}, bf16[128,4096]{1,0:T(8,128)(2,1)S(1)}, u32[]{:S(2)}, u32[]{:S(2)}) %collective-permute-start.9) | collective-permute-done | bytes 1048608 | tf_op jit(solution)/shard_map/ppermute | solution.py:31
  266.1 31.1 %collective-permute-done.10 = bf16[128,4096]{1,0:T(8,128)(2,1)S(1)} collective-permute-done((bf16[128,4096]{1,0:T(8,128)(2,1)S(1)}, bf16[128,4096]{1,0:T(8,128)(2,1)S(1)}, u32[]{:S(2)}, u32[]{:S(2)}) %collective-permute-start.10) | collective-permute-done | bytes 1048608 | tf_op jit(solution)/shard_map/ppermute | solution.py:31
  298.2 49.7 %collective-permute-done.11 = bf16[128,4096]{1,0:T(8,128)(2,1)S(1)} collective-permute-done((bf16[128,4096]{1,0:T(8,128)(2,1)S(1)}, bf16[128,4096]{1,0:T(8,128)(2,1)S(1)}, u32[]{:S(2)}, u32[]{:S(2)}) %collective-permute-start.11) | collective-permute-done | bytes 1048608 | tf_op jit(solution)/shard_map/ppermute | solution.py:31
  348.8 49.7 %collective-permute-done.12 = bf16[128,4096]{1,0:T(8,128)(2,1)S(1)} collective-permute-done((bf16[128,4096]{1,0:T(8,128)(2,1)S(1)}, bf16[128,4096]{1,0:T(8,128)(2,1)S(1)}, u32[]{:S(2)}, u32[]{:S(2)}) %collective-permute-start.12) | collective-permute-done | bytes 1048608 | tf_op jit(solution)/shard_map/ppermute | solution.py:31
  399.5 23.1 %collective-permute-done.13 = bf16[128,4096]{1,0:T(8,128)(2,1)} collective-permute-done((bf16[128,4096]{1,0:T(8,128)(2,1)S(1)}, bf16[128,4096]{1,0:T(8,128)(2,1)}, u32[]{:S(2)}, u32[]{:S(2)}) %collective-permute-start.13) | collective-permute-done | bytes 1048608 | tf_op jit(solution)/shard_map/ppermute | solution.py:31
  422.7 44.7 %collective-permute-done.14 = bf16[128,4096]{1,0:T(8,128)(2,1)} collective-permute-done((bf16[128,4096]{1,0:T(8,128)(2,1)}, bf16[128,4096]{1,0:T(8,128)(2,1)}, u32[]{:S(2)}, u32[]{:S(2)}) %collective-permute-start.14) | collective-permute-done | bytes 1048608 | tf_op jit(solution)/shard_map/ppermute | solution.py:31
  467.4 2.3 constant_dynamic-update-slice_fusion.31
  469.7 2.3 constant_dynamic-update-slice_fusion.30
  472.1 2.3 constant_dynamic-update-slice_fusion.29
  474.4 2.3 constant_dynamic-update-slice_fusion.28
  476.7 2.3 constant_dynamic-update-slice_fusion.27
  479.0 2.3 constant_dynamic-update-slice_fusion.26
  481.3 2.3 constant_dynamic-update-slice_fusion.25
  483.6 2.4 constant_dynamic-update-slice_fusion.24
  485.9 2.3 constant_dynamic-update-slice_fusion.23
  488.2 2.3 constant_dynamic-update-slice_fusion.22
  490.5 2.3 constant_dynamic-update-slice_fusion.21
  492.8 2.3 constant_dynamic-update-slice_fusion.20
  495.1 2.3 constant_dynamic-update-slice_fusion.19
  498.4 1.1 constant_dynamic-update-slice_fusion.17
  499.5 1.1 constant_dynamic-update-slice_fusion.16
  500.6 2.3 constant_dynamic-update-slice_fusion.15
  502.9 2.3 constant_dynamic-update-slice_fusion.14
  505.2 1.0 constant_dynamic-update-slice_fusion.13
  506.3 1.1 constant_dynamic-update-slice_fusion.12
  507.3 1.1 constant_dynamic-update-slice_fusion.11
  508.4 1.0 constant_dynamic-update-slice_fusion.10
  510.5 1.1 constant_dynamic-update-slice_fusion.8
  514.7 1.1 constant_dynamic-update-slice_fusion.4
  515.8 2.3 constant_dynamic-update-slice_fusion.3
  519.1 1.1 constant_dynamic-update-slice_fusion.1
  520.2 1.1 constant_dynamic-update-slice_fusion
  521.4 15.4 %fusion.2 = f32[4096,512]{1,0:T(8,128)} fusion(bf16[512,2048]{1,0:T(8,128)(2,1)} %all-gather.4.cloned.1.call-done, bf16[4096,4096]{1,0:T(8,128)(2,1)} %constant_dynamic-update-slice_fusion, s32[]{:T(128)S(6)} %select_n.14), kind=kOutput, calls=%fused_computation.4 | convolution fusion | flops 8589934592 | bytes 27262980 | tf_op jit(solution)/shard_map/dot_general | solution.py:35
  536.7 16.2 %multiply_convert_fusion = bf16[4096,2048]{1,0:T(8,128)(2,1)} fusion(bf16[512,2048]{1,0:T(8,128)(2,1)} %all-gather.6.cloned.1.call-done, f32[4096,512]{1,0:T(8,128)} %fusion.2), kind=kOutput, calls=%fused_computation | convolution fusion | flops 8613003264 | bytes 27262976 | tf_op jit(solution)/shard_map/dot_general | solution.py:14
  552.9 20.7 %copy.14 = bf16[4096,2048]{0,1:T(8,128)(2,1)} copy(bf16[4096,2048]{1,0:T(8,128)(2,1)} %multiply_convert_fusion) | data formatting | bytes 33554432
  573.7 17.5 %fusion.5 = bf16[512,4096]{0,1:T(8,128)(2,1)S(1)} fusion(f32[4096,512]{1,0:T(8,128)} %fusion.2, bf16[512,2048]{1,0:T(8,128)(2,1)} %all-gather.6.cloned.1.call-done, bf16[4096,2048]{1,0:T(8,128)(2,1)} %all-gather.8.cloned.1.call-done), kind=kOutput, calls=%fused_computation.8 | convolution fusion | flops 8598323200 | bytes 31457280 | tf_op jit(solution)/shard_map/dot_general | solution.py:8
  591.2 2.2 copy-done.22
  593.4 11.7 fusion.4
  605.1 20.8 %copy.12 = bf16[2048,4096]{1,0:T(8,128)(2,1)} copy(bf16[2048,4096]{0,1:T(8,128)(2,1)} %fusion.4) | data formatting | bytes 33554432
  626.0 15.1 %fusion.7 = bf16[512,2048]{1,0:T(8,128)(2,1)} fusion(bf16[512,4096]{0,1:T(8,128)(2,1)} %copy-done.22, bf16[4096,4096]{1,0:T(8,128)(2,1)} %constant_dynamic-update-slice_fusion, s32[]{:T(128)S(6)} %select_n.14), kind=kOutput, calls=%fused_computation.11 | convolution fusion | flops 8590983168 | bytes 23068676 | tf_op jit(solution)/shard_map/dot_general | solution.py:8
  641.1 292.0 %reduce-scatter.12.cloned.1.call-done = bf16[128,4096]{1,0:T(8,128)(2,1)} async-done(((bf16[2048,4096]{1,0:T(8,128)(2,1)}), bf16[128,4096]{1,0:T(8,128)(2,1)}) %reduce-scatter.12.cloned.1.call-update) | async-done | bytes 1048592
  933.1 1.6 copy.15
  934.7 1.5 convert_element_type.32
  936.2 351.2 %reduce-scatter.10.cloned.1.call-done = bf16[128,4096]{1,0:T(8,128)(2,1)} async-done(((bf16[2048,4096]{1,0:T(8,128)(2,1)}), bf16[128,4096]{1,0:T(8,128)(2,1)}) %reduce-scatter.10.cloned.1.call-update) | async-done | bytes 1048592
  1287.3 1.6 copy.13
  1289.0 1.6 copy.10
  1290.6 14.7 %reduce-scatter.8.cloned.1.call-done = bf16[512,1024]{1,0:T(8,128)(2,1)} async-done(((bf16[512,2048]{1,0:T(8,128)(2,1)}), bf16[512,1024]{1,0:T(8,128)(2,1)}) %reduce-scatter.8.cloned.1.call-update) | async-done | bytes 1048592 | tf_op jit(solution)/shard_map/reduce_scatter | solution.py:40
  (73 shorter events, 17.3 us)
Async XLA Ops:
  7.2 492.4 %copy-start = (bf16[128,4096]{1,0:T(8,128)(2,1)S(1)}, bf16[128,4096]{1,0:T(8,128)(2,1)}, u32[]{:S(2)}) copy-start(bf16[128,4096]{1,0:T(8,128)(2,1)} %param.6) | copy-start | bytes 3145732
  7.2 514.2 %all-gather.4.cloned.1.call-start = ((), (), s32[]{:S(2)}) async-start(), calls=%async_computation.3 | async-start | bytes 3145728 | tf_op jit(solution)/shard_map/all_gather | solution.py:21
  7.9 528.8 %all-gather.6.cloned.1.call-start = ((), (), s32[]{:S(2)}) async-start(), calls=%async_computation.4 | async-start | bytes 3145728 | tf_op jit(solution)/shard_map/all_gather | solution.py:22
  8.0 30.4 %collective-permute-start = (bf16[128,4096]{1,0:T(8,128)(2,1)}, bf16[128,4096]{1,0:T(8,128)(2,1)S(1)}, u32[]{:S(2)}, u32[]{:S(2)}) collective-permute-start(bf16[128,4096]{1,0:T(8,128)(2,1)} %param.6), channel_id=1, source_target_pairs={{0,2},{2,4},{4,6},{6,8},{8,10},{10,12},{12,14},{14,16},{16,18},{18... | collective-permute-start | bytes 3145736 | tf_op jit(solution)/shard_map/ppermute | solution.py:31
  11.0 562.7 %all-gather.8.cloned.1.call-start = ((), (), s32[]{:S(2)}) async-start(), calls=%async_computation.5 | async-start | bytes 17825792 | tf_op jit(solution)/shard_map/all_gather | solution.py:28
  38.3 27.9 %collective-permute-start.1 = (bf16[128,4096]{1,0:T(8,128)(2,1)S(1)}, bf16[128,4096]{1,0:T(8,128)(2,1)S(1)}, u32[]{:S(2)}, u32[]{:S(2)}) collective-permute-start(bf16[128,4096]{1,0:T(8,128)(2,1)S(1)} %collective-permute-done), channel_id=1, source_target_pairs={{0,2},{2,4},{4,6},{6,8},{8,10},{10,12},{12,14},{14,16},{16,18},{18... | collective-permute-start | bytes 3145736 | tf_op jit(solution)/shard_map/ppermute | solution.py:31
  66.3 33.8 %collective-permute-start.2 = (bf16[128,4096]{1,0:T(8,128)(2,1)S(1)}, bf16[128,4096]{1,0:T(8,128)(2,1)}, u32[]{:S(2)}, u32[]{:S(2)}) collective-permute-start(bf16[128,4096]{1,0:T(8,128)(2,1)S(1)} %collective-permute-done.1), channel_id=1, source_target_pairs={{0,2},{2,4},{4,6},{6,8},{8,10},{10,12},{12,14},{14,16},{16,18},{18... | collective-permute-start | bytes 3145736 | tf_op jit(solution)/shard_map/ppermute | solution.py:31
  66.3 866.8 %reduce-scatter.12.cloned.1.call-start = ((), (), s32[]{:S(2)}) async-start(), calls=%async_computation.8 | async-start | bytes 17825792
  100.0 22.8 %collective-permute-start.3 = (bf16[128,4096]{1,0:T(8,128)(2,1)}, bf16[128,4096]{1,0:T(8,128)(2,1)S(1)}, u32[]{:S(2)}, u32[]{:S(2)}) collective-permute-start(bf16[128,4096]{1,0:T(8,128)(2,1)} %collective-permute-done.2), channel_id=1, source_target_pairs={{0,2},{2,4},{4,6},{6,8},{8,10},{10,12},{12,14},{14,16},{16,18},{18... | collective-permute-start | bytes 3145736 | tf_op jit(solution)/shard_map/ppermute | solution.py:31
  122.8 1.0 copy-start.1
  123.8 22.4 %collective-permute-start.4 = (bf16[128,4096]{1,0:T(8,128)(2,1)S(1)}, bf16[128,4096]{1,0:T(8,128)(2,1)S(1)}, u32[]{:S(2)}, u32[]{:S(2)}) collective-permute-start(bf16[128,4096]{1,0:T(8,128)(2,1)S(1)} %collective-permute-done.3), channel_id=1, source_target_pairs={{0,2},{2,4},{4,6},{6,8},{8,10},{10,12},{12,14},{14,16},{16,18},{18... | collective-permute-start | bytes 3145736 | tf_op jit(solution)/shard_map/ppermute | solution.py:31
  146.2 1.0 copy-start.3
  147.2 22.4 %collective-permute-start.5 = (bf16[128,4096]{1,0:T(8,128)(2,1)S(1)}, bf16[128,4096]{1,0:T(8,128)(2,1)S(1)}, u32[]{:S(2)}, u32[]{:S(2)}) collective-permute-start(bf16[128,4096]{1,0:T(8,128)(2,1)S(1)} %collective-permute-done.4), channel_id=1, source_target_pairs={{0,2},{2,4},{4,6},{6,8},{8,10},{10,12},{12,14},{14,16},{16,18},{18... | collective-permute-start | bytes 3145736 | tf_op jit(solution)/shard_map/ppermute | solution.py:31
  169.6 1.0 copy-start.5
  170.6 22.4 %collective-permute-start.6 = (bf16[128,4096]{1,0:T(8,128)(2,1)S(1)}, bf16[128,4096]{1,0:T(8,128)(2,1)S(1)}, u32[]{:S(2)}, u32[]{:S(2)}) collective-permute-start(bf16[128,4096]{1,0:T(8,128)(2,1)S(1)} %collective-permute-done.5), channel_id=1, source_target_pairs={{0,2},{2,4},{4,6},{6,8},{8,10},{10,12},{12,14},{14,16},{16,18},{18... | collective-permute-start | bytes 3145736 | tf_op jit(solution)/shard_map/ppermute | solution.py:31
  193.1 1.0 copy-start.7
  194.1 22.4 %collective-permute-start.7 = (bf16[128,4096]{1,0:T(8,128)(2,1)S(1)}, bf16[128,4096]{1,0:T(8,128)(2,1)S(1)}, u32[]{:S(2)}, u32[]{:S(2)}) collective-permute-start(bf16[128,4096]{1,0:T(8,128)(2,1)S(1)} %collective-permute-done.6), channel_id=1, source_target_pairs={{0,2},{2,4},{4,6},{6,8},{8,10},{10,12},{12,14},{14,16},{16,18},{18... | collective-permute-start | bytes 3145736 | tf_op jit(solution)/shard_map/ppermute | solution.py:31
  216.5 1.0 copy-start.9
  217.5 22.6 %collective-permute-start.8 = (bf16[128,4096]{1,0:T(8,128)(2,1)S(1)}, bf16[128,4096]{1,0:T(8,128)(2,1)S(1)}, u32[]{:S(2)}, u32[]{:S(2)}) collective-permute-start(bf16[128,4096]{1,0:T(8,128)(2,1)S(1)} %collective-permute-done.7), channel_id=1, source_target_pairs={{0,2},{2,4},{4,6},{6,8},{8,10},{10,12},{12,14},{14,16},{16,18},{18... | collective-permute-start | bytes 3145736 | tf_op jit(solution)/shard_map/ppermute | solution.py:31
  240.1 1.0 copy-start.11
  241.1 23.8 %collective-permute-start.9 = (bf16[128,4096]{1,0:T(8,128)(2,1)S(1)}, bf16[128,4096]{1,0:T(8,128)(2,1)S(1)}, u32[]{:S(2)}, u32[]{:S(2)}) collective-permute-start(bf16[128,4096]{1,0:T(8,128)(2,1)S(1)} %collective-permute-done.8), channel_id=1, source_target_pairs={{0,2},{2,4},{4,6},{6,8},{8,10},{10,12},{12,14},{14,16},{16,18},{18... | collective-permute-start | bytes 3145736 | tf_op jit(solution)/shard_map/ppermute | solution.py:31
  264.9 1.0 copy-start.13
  265.9 31.3 %collective-permute-start.10 = (bf16[128,4096]{1,0:T(8,128)(2,1)S(1)}, bf16[128,4096]{1,0:T(8,128)(2,1)S(1)}, u32[]{:S(2)}, u32[]{:S(2)}) collective-permute-start(bf16[128,4096]{1,0:T(8,128)(2,1)S(1)} %collective-permute-done.9), channel_id=1, source_target_pairs={{0,2},{2,4},{4,6},{6,8},{8,10},{10,12},{12,14},{14,16},{16,18},{18... | collective-permute-start | bytes 3145736 | tf_op jit(solution)/shard_map/ppermute | solution.py:31
  297.2 1.0 copy-start.15
  298.2 49.7 %collective-permute-start.11 = (bf16[128,4096]{1,0:T(8,128)(2,1)S(1)}, bf16[128,4096]{1,0:T(8,128)(2,1)S(1)}, u32[]{:S(2)}, u32[]{:S(2)}) collective-permute-start(bf16[128,4096]{1,0:T(8,128)(2,1)S(1)} %collective-permute-done.10), channel_id=1, source_target_pairs={{0,2},{2,4},{4,6},{6,8},{8,10},{10,12},{12,14},{14,16},{16,18},{18... | collective-permute-start | bytes 3145736 | tf_op jit(solution)/shard_map/ppermute | solution.py:31
  347.9 1.0 copy-start.17
  348.8 49.7 %collective-permute-start.12 = (bf16[128,4096]{1,0:T(8,128)(2,1)S(1)}, bf16[128,4096]{1,0:T(8,128)(2,1)S(1)}, u32[]{:S(2)}, u32[]{:S(2)}) collective-permute-start(bf16[128,4096]{1,0:T(8,128)(2,1)S(1)} %collective-permute-done.11), channel_id=1, source_target_pairs={{0,2},{2,4},{4,6},{6,8},{8,10},{10,12},{12,14},{14,16},{16,18},{18... | collective-permute-start | bytes 3145736 | tf_op jit(solution)/shard_map/ppermute | solution.py:31
  398.5 1.0 copy-start.19
  399.5 23.1 %collective-permute-start.13 = (bf16[128,4096]{1,0:T(8,128)(2,1)S(1)}, bf16[128,4096]{1,0:T(8,128)(2,1)}, u32[]{:S(2)}, u32[]{:S(2)}) collective-permute-start(bf16[128,4096]{1,0:T(8,128)(2,1)S(1)} %collective-permute-done.12), channel_id=1, source_target_pairs={{0,2},{2,4},{4,6},{6,8},{8,10},{10,12},{12,14},{14,16},{16,18},{18... | collective-permute-start | bytes 3145736 | tf_op jit(solution)/shard_map/ppermute | solution.py:31
  422.6 44.8 %collective-permute-start.14 = (bf16[128,4096]{1,0:T(8,128)(2,1)}, bf16[128,4096]{1,0:T(8,128)(2,1)}, u32[]{:S(2)}, u32[]{:S(2)}) collective-permute-start(bf16[128,4096]{1,0:T(8,128)(2,1)} %collective-permute-done.13), channel_id=1, source_target_pairs={{0,2},{2,4},{4,6},{6,8},{8,10},{10,12},{12,14},{14,16},{16,18},{18... | collective-permute-start | bytes 3145736 | tf_op jit(solution)/shard_map/ppermute | solution.py:31
  422.6 82.6 %copy-start.20 = (bf16[128,4096]{1,0:T(8,128)(2,1)S(1)}, bf16[128,4096]{1,0:T(8,128)(2,1)}, u32[]{:S(2)}) copy-start(bf16[128,4096]{1,0:T(8,128)(2,1)} %copy-done.19) | copy-start | bytes 3145732
  422.6 83.7 %copy-start.18 = (bf16[128,4096]{1,0:T(8,128)(2,1)S(1)}, bf16[128,4096]{1,0:T(8,128)(2,1)}, u32[]{:S(2)}) copy-start(bf16[128,4096]{1,0:T(8,128)(2,1)} %copy-done.17) | copy-start | bytes 3145732
  422.6 84.7 %copy-start.16 = (bf16[128,4096]{1,0:T(8,128)(2,1)S(1)}, bf16[128,4096]{1,0:T(8,128)(2,1)}, u32[]{:S(2)}) copy-start(bf16[128,4096]{1,0:T(8,128)(2,1)} %copy-done.15) | copy-start | bytes 3145732
  422.6 85.8 %copy-start.14 = (bf16[128,4096]{1,0:T(8,128)(2,1)S(1)}, bf16[128,4096]{1,0:T(8,128)(2,1)}, u32[]{:S(2)}) copy-start(bf16[128,4096]{1,0:T(8,128)(2,1)} %copy-done.13) | copy-start | bytes 3145732
  422.6 86.8 %copy-start.12 = (bf16[128,4096]{1,0:T(8,128)(2,1)S(1)}, bf16[128,4096]{1,0:T(8,128)(2,1)}, u32[]{:S(2)}) copy-start(bf16[128,4096]{1,0:T(8,128)(2,1)} %copy-done.11) | copy-start | bytes 3145732
  422.6 87.9 %copy-start.10 = (bf16[128,4096]{1,0:T(8,128)(2,1)S(1)}, bf16[128,4096]{1,0:T(8,128)(2,1)}, u32[]{:S(2)}) copy-start(bf16[128,4096]{1,0:T(8,128)(2,1)} %copy-done.9) | copy-start | bytes 3145732
  422.6 89.0 %copy-start.8 = (bf16[128,4096]{1,0:T(8,128)(2,1)S(1)}, bf16[128,4096]{1,0:T(8,128)(2,1)}, u32[]{:S(2)}) copy-start(bf16[128,4096]{1,0:T(8,128)(2,1)} %copy-done.7) | copy-start | bytes 3145732
  422.6 90.0 %copy-start.6 = (bf16[128,4096]{1,0:T(8,128)(2,1)S(1)}, bf16[128,4096]{1,0:T(8,128)(2,1)}, u32[]{:S(2)}) copy-start(bf16[128,4096]{1,0:T(8,128)(2,1)} %copy-done.5) | copy-start | bytes 3145732
  422.7 91.0 %copy-start.4 = (bf16[128,4096]{1,0:T(8,128)(2,1)S(1)}, bf16[128,4096]{1,0:T(8,128)(2,1)}, u32[]{:S(2)}) copy-start(bf16[128,4096]{1,0:T(8,128)(2,1)} %copy-done.3) | copy-start | bytes 3145732
  422.7 92.1 %copy-start.2 = (bf16[128,4096]{1,0:T(8,128)(2,1)S(1)}, bf16[128,4096]{1,0:T(8,128)(2,1)}, u32[]{:S(2)}) copy-start(bf16[128,4096]{1,0:T(8,128)(2,1)} %copy-done.1) | copy-start | bytes 3145732
  573.6 19.8 %copy-start.21 = (bf16[512,2048]{1,0:T(8,128)(2,1)S(1)}, bf16[512,2048]{1,0:T(8,128)(2,1)}, u32[]{:S(2)}) copy-start(bf16[512,2048]{1,0:T(8,128)(2,1)} %all-gather.4.cloned.1.call-done) | copy-start | bytes 6291460
  573.6 713.7 %reduce-scatter.10.cloned.1.call-start = ((), (), s32[]{:S(2)}) async-start(), calls=%async_computation.7 | async-start | bytes 17825792
  591.2 2.2 copy-start.22
  625.9 679.4 %reduce-scatter.8.cloned.1.call-start = ((), (), s32[]{:S(2)}) async-start(), calls=%async_computation.6 | async-start | bytes 3145728 | tf_op jit(solution)/shard_map/reduce_scatter | solution.py:40
Sparse Core Ops, SparseCore 0:
  9.5 13.2 all-gather.3
  24.4 11.7 all-gather.5
  66.4 498.3 all-gather.7
  573.7 359.3 reduce-scatter.11
  935.3 352.0 reduce-scatter.9
  1290.0 15.2 reduce-scatter.7
